TPU v7x, 32 devices: a whole 2x2x4 slice. The times are simulated.
32 devices in a mesh: sp: 8 (over z, x), tp: 4 (over y, core).
Axes of the slice: x: 2, y: 2, z: 4, core: 2. Of those that a mesh axis runs over, the one named last changes fastest.
Arguments:
- tokens: bfloat16 [2048, 4096], P('sp', 'tp'), may hold values from -6 to 6
- pre_gain: float32 [4096], replicated, may hold values from 0.1 to 1.9
- rate_factor: float32 [2048], P('sp'), may hold values from 0.5 to 2, as said below
- w_rec_in: bfloat16 [4096, 1024], P(None, 'tp'), may hold values from -0.09375 to 0.09375
- w_rec_gate: bfloat16 [4096, 1024], P(None, 'tp')
- conv_taps: float32 [4, 1024], P(None, 'tp'), may hold values from -3 to 3
- rate_maps: bfloat16 [8, 128, 128], P('tp'), may hold values from -0.5 to 0.5
- input_maps: bfloat16 [8, 128, 128], P('tp'), may hold values from -0.5 to 0.5
- decay_param: float32 [1024], P('tp'), as said below
- w_query: bfloat16 [4096, 1536], P(None, 'tp'), may hold values from -0.09375 to 0.09375
- w_latent: bfloat16 [4096, 512], replicated, may hold values from -0.09375 to 0.09375
- w_rope_key: bfloat16 [4096, 64], replicated, may hold values from -0.09375 to 0.09375
- latent_gain: float32 [512], replicated, may hold values from 0.7 to 100, as said below
- w_expand: bfloat16 [512, 2048], P(None, 'tp')
- rec_gain: float32 [1024], P('tp'), may hold values from 0.1 to 1.9
- att_gain: float32 [1024], P('tp'), may hold values from 0.1 to 1.9
- w_out_rec: bfloat16 [1024, 4096], P('tp'), may hold values from -0.125 to 0.125
- w_out_att: bfloat16 [1024, 4096], P('tp'), may hold values from -0.125 to 0.125
- post_gain: float32 [4096], replicated, may hold values from 0.1 to 1.9
Outputs:
- layer_out: bfloat16 [2048, 4096], P(('sp', 'tp'))
Inputs may be any that keep to these rules, and one draw needn't show every extreme that they name: `rate_factor`: one positive factor for each position. `decay_param`: one parameter for each recurrent channel. `latent_gain`: one positive gain for each latent entry.
All inputs are finite; a program needn't handle non-finite values.
Results may differ from a plain program's by a relative error of at most 0.017.
The roundings to bfloat16 on the way count: a program that leaves them out, or rounds other values in their place, can miss the bound.
Values may be sent and summed in bfloat16 or wider, within the bound.
No kernel may reach another device: no remote copies, remote signals or barrier semaphores. Data moves between devices by JAX's collectives and lax.ppermute only.
A program may use at most 128 MiB of HBM per device.

v0:
```python
import math
import jax
import jax.numpy as jnp
from jax import lax
from jax.sharding import PartitionSpec as P

NOPE = 128
ROPE = 64
VDIM = 128
EPS = 1e-06
RATE_C = 8.0
THETA = 10000.0
span_limit = 2048


def passed_along(block, axis, distance):
    devices = range(lax.axis_size(axis))
    route = [(i - distance, i) for i in devices if i - distance in devices]
    return lax.ppermute(block, axis, route)


def entering(value, axis, join, neutral):
    count, mine = (lax.axis_size(axis), lax.axis_index(axis))
    pieces = jax.tree.map(lambda part: lax.all_gather(part, axis), value)
    subtotal = jax.tree.map(
        lambda part, zero: jnp.full_like(part, 0) + jnp.asarray(zero, part.dtype), value, neutral
    )

    def step(position, subtotal):
        longer = join(subtotal, jax.tree.map(lambda part: part[position], pieces))
        return jax.tree.map(lambda new, old: jnp.where(position < mine, new, old), longer, subtotal)

    return lax.fori_loop(0, count - 1, step, subtotal)


def rms_inverse(values):
    return lax.rsqrt(jnp.mean(values * values, axis=-1, keepdims=True) + EPS)


def rotate(values, cosine, sine_part):
    half_width = values.shape[-1] // 2
    leading = values[..., :half_width]
    trailing = values[..., half_width:]
    return jnp.concatenate(
        [leading * cosine - trailing * sine_part, trailing * cosine + leading * sine_part], axis=-1
    )


def angles(length, offset, span_width):
    frequency = 1.0 / THETA ** (jnp.arange(0, span_width, 2).astype(jnp.float32) / span_width)
    places = (offset + jnp.arange(length)).astype(jnp.float32)
    turned = places[:, None] * frequency[None, :]
    return (jnp.cos(turned), jnp.sin(turned))


def combine_steps(earlier, later):
    return (earlier[0] * later[0], later[0] * earlier[1] + later[1])


def attend_block(state_now, query_nope, query_rope, places, keys_nope, key_rope, values, key_root):
    maxima, totals, accumulated = state_now
    scaling = 1.0 / math.sqrt(query_nope.shape[-1] + query_rope.shape[-1])
    scores = jnp.einsum("qhd,khd->hqk", query_nope, keys_nope, preferred_element_type=jnp.float32)
    scores = scores + jnp.einsum(
        "qhd,kd->hqk", query_rope, key_rope, preferred_element_type=jnp.float32
    )
    scores = scores * scaling
    key_places = key_root + jnp.arange(keys_nope.shape[0])
    visible = key_places[None, :] <= places[:, None]
    scores = jnp.where(visible[None], scores, -jnp.inf)
    largest = jnp.maximum(maxima, jnp.max(scores, axis=-1))
    anchor = jnp.where(largest == -jnp.inf, 0.0, largest)
    weights = jnp.exp(scores - anchor[..., None])
    shrink = jnp.exp(maxima - anchor)
    totals = totals * shrink + jnp.sum(weights, axis=-1)
    accumulated = accumulated * shrink[..., None] + jnp.einsum(
        "hqk,khd->hqd", weights.astype(jnp.bfloat16), values, preferred_element_type=jnp.float32
    )
    return (largest, totals, accumulated)


def shards(
    tokens,
    pre_gain,
    rate_factor,
    w_rec_in,
    w_rec_gate,
    conv_taps,
    rate_maps,
    input_maps,
    decay_param,
    w_query,
    w_latent,
    w_rope_key,
    latent_gain,
    w_expand,
    rec_gain,
    att_gain,
    w_out_rec,
    w_out_att,
    post_gain,
):
    row_count = tokens.shape[0]
    model_width = w_rec_in.shape[0]
    channels = w_rec_in.shape[1]
    heads_here = w_query.shape[1] // (NOPE + ROPE)
    group_size = lax.axis_size("tp")
    first_place = lax.axis_index("sp") * row_count
    places = first_place + jnp.arange(row_count)
    last_place = first_place + row_count - 1
    piece_wide = lax.all_gather(tokens, "tp", axis=1, tiled=True).astype(jnp.float32)
    piece_low = (piece_wide * pre_gain).astype(jnp.bfloat16)

    def accumulate(source, weight):
        return jnp.dot(source, weight, preferred_element_type=jnp.float32)

    squares = jnp.sum(piece_wide * piece_wide, axis=1, keepdims=True)
    sum_input = accumulate(piece_low, w_rec_in)
    sum_gate = accumulate(piece_low, w_rec_gate)
    sum_query = accumulate(piece_low, w_query)
    sum_latent = accumulate(piece_low, w_latent)
    sum_rope = accumulate(piece_low, w_rope_key)
    inverse = lax.rsqrt(squares / model_width + EPS)
    rec_input = (inverse * sum_input).astype(jnp.bfloat16)
    gate_value = inverse * sum_gate
    query_raw = inverse * sum_query
    latent_raw = inverse * sum_latent
    rope_raw = inverse * sum_rope
    taps = conv_taps.shape[0]
    tail_rows = rec_input[row_count - (taps - 1) :]
    before = passed_along(tail_rows, "sp", 1)
    padded = jnp.concatenate([before, rec_input], axis=0)
    convolved = conv_taps[0] * padded[0:row_count].astype(jnp.float32)
    for tap_index in range(1, taps):
        convolved = convolved + conv_taps[tap_index] * padded[
            tap_index : tap_index + row_count
        ].astype(jnp.float32)
    conv_low = convolved.astype(jnp.bfloat16)
    blocks = conv_low.reshape(row_count, rate_maps.shape[0], rate_maps.shape[1])
    rate_gate = jax.nn.sigmoid(
        jnp.einsum("sbi,bij->sbj", blocks, rate_maps, preferred_element_type=jnp.float32)
    ).reshape(row_count, channels)
    entry_gate = jax.nn.sigmoid(
        jnp.einsum("sbi,bij->sbj", blocks, input_maps, preferred_element_type=jnp.float32)
    ).reshape(row_count, channels)
    log_keep = -RATE_C * rate_factor[:, None] * rate_gate * jax.nn.softplus(-decay_param)
    keep_rate = jnp.exp(log_keep)
    driven = jnp.sqrt(-jnp.expm1(2.0 * log_keep)) * entry_gate * convolved
    cum_keep, local_state = lax.associative_scan(combine_steps, (keep_rate, driven), axis=0)
    identity = (jnp.ones((channels,), jnp.float32), jnp.zeros((channels,), jnp.float32))
    chain_keep, carried = entering(
        (cum_keep[row_count - 1], local_state[row_count - 1]), "sp", combine_steps, identity
    )
    state_seq = local_state + cum_keep * carried[None, :]
    rec_out = state_seq * jax.nn.gelu(gate_value)
    rec_squares = jnp.sum(rec_out * rec_out, axis=1, keepdims=True)
    cosine, sine_part = angles(row_count, first_place, ROPE)
    query_heads = query_raw.reshape(row_count, heads_here, NOPE + ROPE)
    query_nope = query_heads[:, :, :NOPE].astype(jnp.bfloat16)
    query_rope = rotate(query_heads[:, :, NOPE:], cosine[:, None, :], sine_part[:, None, :]).astype(
        jnp.bfloat16
    )
    own_latent = (latent_raw * rms_inverse(latent_raw) * latent_gain).astype(jnp.bfloat16)
    rope_key = rotate(rope_raw, cosine, sine_part).astype(jnp.bfloat16)
    start_state = (
        jnp.full((heads_here, row_count), -jnp.inf, jnp.float32),
        jnp.zeros((heads_here, row_count), jnp.float32),
        jnp.zeros((heads_here, row_count, VDIM), jnp.float32),
    )
    expanded_local = jnp.dot(own_latent, w_expand, preferred_element_type=jnp.float32).astype(
        jnp.bfloat16
    )
    key_source = lax.all_gather(expanded_local, "sp", axis=0, tiled=True)
    rope_source = lax.all_gather(rope_key, "sp", axis=0, tiled=True)
    total_rows = key_source.shape[0]
    key_span = math.gcd(total_rows, span_limit)

    def one_span(span_index, state_inner):
        key_root = span_index * key_span

        def compute(state_deep):
            source_rows = lax.dynamic_slice_in_dim(key_source, span_index * key_span, key_span, 0)
            rope_rows = lax.dynamic_slice_in_dim(rope_source, span_index * key_span, key_span, 0)
            expanded = source_rows
            expanded = expanded.reshape(key_span, heads_here, NOPE + VDIM)
            return attend_block(
                state_deep,
                query_nope,
                query_rope,
                places,
                expanded[:, :, :NOPE],
                rope_rows,
                expanded[:, :, NOPE:],
                key_root,
            )

        def keep_state(state_deep):
            return state_deep

        return lax.cond(key_root <= last_place, compute, keep_state, state_inner)

    maxima, totals, accumulated = lax.fori_loop(0, total_rows // key_span, one_span, start_state)
    att_out = (
        (accumulated / totals[..., None]).transpose(1, 0, 2).reshape(row_count, heads_here * VDIM)
    )
    att_squares = jnp.sum(att_out * att_out, axis=1, keepdims=True)
    rec_total, att_total = lax.psum((rec_squares, att_squares), "tp")
    rec_norm = (rec_out * lax.rsqrt(rec_total / (channels * group_size) + EPS) * rec_gain).astype(
        jnp.bfloat16
    )
    att_norm = (
        att_out * lax.rsqrt(att_total / (heads_here * VDIM * group_size) + EPS) * att_gain
    ).astype(jnp.bfloat16)
    mixed_sum = lax.psum_scatter(
        (
            jnp.dot(rec_norm, w_out_rec, preferred_element_type=jnp.float32)
            + jnp.dot(att_norm, w_out_att, preferred_element_type=jnp.float32)
        ).astype(jnp.bfloat16),
        "tp",
        scatter_dimension=0,
        tiled=True,
    ).astype(jnp.float32)
    return (mixed_sum * rms_inverse(mixed_sum) * post_gain).astype(jnp.bfloat16)


def solution(mesh):
    placed = (
        P("sp", "tp"),
        P(),
        P("sp"),
        P(None, "tp"),
        P(None, "tp"),
        P(None, "tp"),
        P("tp", None, None),
        P("tp", None, None),
        P("tp"),
        P(None, "tp"),
        P(),
        P(),
        P(),
        P(None, "tp"),
        P("tp"),
        P("tp"),
        P("tp", None),
        P("tp", None),
        P(),
    )
    return jax.shard_map(
        shards, mesh=mesh, in_specs=placed, out_specs=P(("sp", "tp"), None), check_vma=False
    )
```

profile of v0, /device:TPU:0, one launch (start us, length us, event | category | flops | bytes accessed | tf_op | source)
XLA Modules:
  0.0 334.9 jit_solution(9606723761074546730)
XLA Ops:
  11.2 23.0 %all-gather.5.cloned.1.call-done = bf16[256,4096]{1,0:T(8,128)(2,1)} async-done(((bf16[256,1024]{1,0:T(8,128)(2,1)}), bf16[256,4096]{1,0:T(8,128)(2,1)}) %all-gather.5.cloned.1.call-update) | async-done | bytes 2097168 | tf_op jit(solution)/shard_map/all_gather | solution.py:111
  34.2 2.2 fusion.15
  36.5 2.5 fusion.23
  39.6 4.1 %collective-permute-start = (bf16[3,256]{1,0:T(4,128)(2,1)}, bf16[3,256]{1,0:T(4,128)(2,1)}, u32[]{:S(2)}, u32[]{:S(2)}) collective-permute-start(bf16[3,256]{1,0:T(4,128)(2,1)} %slice.384), channel_id=1, source_target_pairs={{0,4},{4,8},{8,12},{12,16},{16,20},{20,24},{24,28},{1,5},{5,9},{9,... | collective-permute-start | bytes 4616 | tf_op jit(solution)/shard_map/ppermute | solution.py:19
  46.3 3.6 %convolution_multiply_fusion.1 = f32[256,384]{1,0:T(8,128)} fusion(bf16[4096,384]{1,0:T(8,128)(2,1)S(1)} %copy-done, bf16[256,4096]{1,0:T(8,128)(2,1)} %all-gather.5.cloned.1.call-done, f32[4096]{0:T(1024)} %param.24, f32[256]{0:T(256)} %copy-done.20), kind=kOutput, calls=%fused_computation.32 | convolution fusion | flops 808550400 | bytes 5653504 | tf_op jit(solution)/shard_map/dot_general | solution.py:115
  51.8 2.6 convolution_multiply_fusion.4
  54.6 33.6 %all_gather.19 = bf16[2048,64]{0,1:T(8,128)(2,1)} all-gather(bf16[256,64]{0,1:T(8,128)(2,1)S(1)} %pad_maximum_fusion.8), channel_id=1, replica_groups=mesh['sp'=8,'tp'=4] {'sp'}, dimensions={0}, use_global_device_ids=true | all-gather | bytes 294912 | tf_op jit(solution)/shard_map/all_gather | solution.py:174
  98.5 2.2 multiply_multiply_fusion.1
  199.9 2.0 pad.124
  207.9 2.2 pad.127
  211.7 2.3 pad.129
  214.0 2.2 pad.111
  217.6 2.1 pad.110
  225.5 17.7 %all-gather = f32[8,1,256]{2,1,0:T(1,128)S(1)} all-gather(f32[1,1,256]{2,1,0:T(1,128)S(1)} %add_bitcast_fusion.1), channel_id=1, replica_groups=mesh['sp'=8,'tp'=4] {'sp'}, dimensions={0}, use_global_device_ids=true | all-gather | bytes 9216 | tf_op jit(solution)/shard_map/all_gather | solution.py:24
  243.2 2.3 pad.113
  248.7 17.0 %all-gather.1 = f32[8,1,256]{2,1,0:T(1,128)S(1)} all-gather(f32[1,1,256]{2,1,0:T(1,128)S(1)} %add_bitcast_fusion), channel_id=1, replica_groups=mesh['sp'=8,'tp'=4] {'sp'}, dimensions={0}, use_global_device_ids=true | all-gather | bytes 9216 | tf_op jit(solution)/shard_map/all_gather | solution.py:24
  266.1 4.0 %multiply_reduce_fusion.1 = (f32[256]{0:T(256)S(1)}, f32[256,256]{1,0:T(8,128)}) fusion(bf16[4096,256]{1,0:T(8,128)(2,1)} %param.27, bf16[256,4096]{1,0:T(8,128)(2,1)} %all-gather.5.cloned.1.call-done, f32[4096]{0:T(1024)} %param.24, f32[256]{0:T(256)} %copy-done.20, f32[256]{0:T(256)S(1)} %get-tuple-element.224, f32[256,256]{1,0:T(8,128)} %pad.128, ...), kind=kOutput, calls=%fused_computation.67 | convolution fusion | flops 541064960 | bytes 5524480 | tf_op jit(solution)/shard_map/dot_general | solution.py:115
  270.1 14.6 %conditional.1 = (f32[2,256]{1,0:T(2,128)S(1)}, f32[2,256,128]{1,2,0:T(8,128)}) conditional(s32[]{:T(128)} %convert_element_type.81, (f32[2,256]{1,0:T(2,128)S(1)}, f32[2,256,128]{2,1,0:T(8,128)S(1)}) %tuple.113, (s32[]{:T(128)}, s32[256]{0:T(256)S(1)}, bf16[2048,512]{1,0:T(8,128)(2,1)}, f32[256,2,192]{0,2,1:T(8,128)}, bf16[2048,64]{0,1:T(8,128)(2,1)}, ...), branch_computations={%region_6.7_spmd, %region_7.10_spmd} | conditional | flops 680135424 | bytes 39873612 | solution.py:200
  270.1 4.0 %copy.56 = bf16[2048,512]{0,1:T(8,128)(2,1)} copy(bf16[2048,512]{1,0:T(8,128)(2,1)} %get-tuple-element.265) | data formatting | bytes 4194304 | tf_op jit(solution)/shard_map
  276.0 2.0 fusion.11
  285.7 5.7 %all-reduce.32 = (f32[256,1]{0,1:T(1,128)S(1)}, f32[256,1]{0,1:T(1,128)S(1)}) all-reduce(f32[256,1]{0,1:T(1,128)S(1)} %bitcast.90, f32[256,1]{0,1:T(1,128)S(1)} %bitcast.84), channel_id=1, replica_groups=mesh['sp'=8,'tp'=4] {'tp'}, use_global_device_ids=true, to_apply=%region_4.5 | all-reduce | flops 512 | bytes 4096 | tf_op jit(solution)/shard_map/psum | solution.py:207
  291.5 2.6 fusion.52
  294.1 2.1 fusion.14
  296.2 28.9 %reduce-scatter.2.cloned.1.call-done = bf16[64,4096]{1,0:T(8,128)(2,1)} async-done(((bf16[256,4096]{1,0:T(8,128)(2,1)}), bf16[64,4096]{1,0:T(8,128)(2,1)}) %reduce-scatter.2.cloned.1.call-update) | async-done | bytes 524304 | tf_op jit(solution)/shard_map/reduce_scatter | solution.py:214
  (233 shorter events, 150.5 us)
Async XLA Ops:
  6.5 39.7 %copy-start = (bf16[4096,384]{1,0:T(8,128)(2,1)S(1)}, bf16[4096,384]{1,0:T(8,128)(2,1)}, u32[]{:S(2)}) copy-start(bf16[4096,384]{1,0:T(8,128)(2,1)} %param.32) | copy-start | bytes 9437188
  6.5 27.7 %all-gather.5.cloned.1.call-start = ((), (), s32[]{:S(2)}) async-start(), calls=%async_computation.1 | async-start | bytes 2621440 | tf_op jit(solution)/shard_map/all_gather | solution.py:111
  7.3 262.8 %all-gather.7.cloned.1.call-start = ((), (), s32[]{:S(2)}) async-start(), calls=%async_computation.2 | async-start | bytes 2359296 | tf_op jit(solution)/shard_map/all_gather | solution.py:173
  36.5 7.2 %copy-start.20 = (f32[256]{0:T(256)}, f32[256]{0:T(256)S(1)}, u32[]{:S(2)}) copy-start(f32[256]{0:T(256)S(1)} %add_rsqrt_fusion.3) | copy-start | bytes 3076
  36.5 7.2 %copy-start.22 = (bf16[4096,512]{1,0:T(8,128)(2,1)S(1)}, bf16[4096,512]{1,0:T(8,128)(2,1)}, u32[]{:S(2)}) copy-start(bf16[4096,512]{1,0:T(8,128)(2,1)} %param.33) | copy-start | bytes 12582916
  36.5 7.2 %copy-start.24 = (f32[4096]{0:T(1024)S(1)}, f32[4096]{0:T(1024)}, u32[]{:S(2)}) copy-start(f32[4096]{0:T(1024)} %param.24) | copy-start | bytes 49156
  39.6 5.5 %copy-start.5 = (bf16[512,512]{1,0:T(8,128)(2,1)S(1)}, bf16[512,512]{1,0:T(8,128)(2,1)}, u32[]{:S(2)}) copy-start(bf16[512,512]{1,0:T(8,128)(2,1)} %param.36) | copy-start | bytes 1572868
  39.6 5.5 %copy-start.17 = (f32[512]{0:T(512)S(1)}, f32[512]{0:T(512)}, u32[]{:S(2)}) copy-start(f32[512]{0:T(512)} %param.35) | copy-start | bytes 6148
  39.6 50.2 %collective-permute-start = (bf16[3,256]{1,0:T(4,128)(2,1)}, bf16[3,256]{1,0:T(4,128)(2,1)}, u32[]{:S(2)}, u32[]{:S(2)}) collective-permute-start(bf16[3,256]{1,0:T(4,128)(2,1)} %slice.384), channel_id=1, source_target_pairs={{0,4},{4,8},{8,12},{12,16},{16,20},{20,24},{24,28},{1,5},{5,9},{9,... | collective-permute-start | bytes 4616 | tf_op jit(solution)/shard_map/ppermute | solution.py:19
  46.2 278.9 %reduce-scatter.2.cloned.1.call-start = ((), (), s32[]{:S(2)}) async-start(), calls=%async_computation.3 | async-start | bytes 2621440 | tf_op jit(solution)/shard_map/reduce_scatter | solution.py:214
  51.8 2.6 copy-start.19
  51.8 2.6 copy-start.21
  51.8 38.0 %copy-start.15 = (f32[1,256]{1,0:T(1,128)S(1)}, f32[1,256]{1,0:T(1,128)}, u32[]{:S(2)}) copy-start(f32[1,256]{1,0:T(1,128)} %get-tuple-element.332) | copy-start | bytes 3076
  51.8 38.0 %copy-start.16 = (f32[1,256]{1,0:T(1,128)S(1)}, f32[1,256]{1,0:T(1,128)}, u32[]{:S(2)}) copy-start(f32[1,256]{1,0:T(1,128)} %get-tuple-element.333) | copy-start | bytes 3076
  51.8 40.3 %copy-start.23 = (bf16[2,128,128]{2,1,0:T(8,128)(2,1)S(1)}, bf16[2,128,128]{2,1,0:T(8,128)(2,1)}, u32[]{:S(2)}) copy-start(bf16[2,128,128]{2,1,0:T(8,128)(2,1)} %param.30) | copy-start | bytes 196612
  191.6 24.5 %copy-start.14 = (f32[1,256]{1,0:T(1,128)S(1)}, f32[1,256]{1,0:T(1,128)}, u32[]{:S(2)}) copy-start(f32[1,256]{1,0:T(1,128)} %slice.390) | copy-start | bytes 3076
  202.0 21.3 %copy-start.13 = (f32[1,256]{1,0:T(1,128)S(1)}, f32[1,256]{1,0:T(1,128)}, u32[]{:S(2)}) copy-start(f32[1,256]{1,0:T(1,128)} %slice.415) | copy-start | bytes 3076
  207.0 38.6 %copy-start.12 = (f32[1,256]{1,0:T(1,128)S(1)}, f32[1,256]{1,0:T(1,128)}, u32[]{:S(2)}) copy-start(f32[1,256]{1,0:T(1,128)} %slice.389) | copy-start | bytes 3076
  211.7 54.0 %copy-start.8 = (f32[256]{0:T(256)S(1)}, f32[256]{0:T(256)}, u32[]{:S(2)}) copy-start(f32[256]{0:T(256)} %custom-call) | copy-start | bytes 3076
  266.1 4.0 %copy-start.6 = (bf16[256,2,64]{0,2,1:T(8,128)(2,1)S(1)}, bf16[256,2,64]{0,2,1:T(8,128)(2,1)}, u32[]{:S(2)}) copy-start(bf16[256,2,64]{0,2,1:T(8,128)(2,1)} %pad_maximum_fusion.5) | copy-start | bytes 196612
  266.1 4.0 %copy-start.9 = (f32[2,256]{1,0:T(2,128)S(1)}, f32[2,256]{1,0:T(2,128)}, u32[]{:S(2)}) copy-start(f32[2,256]{1,0:T(2,128)} %broadcast_in_dim.63) | copy-start | bytes 6148
  270.1 21.3 %copy-start.18 = (f32[256]{0:T(256)S(1)}, f32[256]{0:T(256)}, u32[]{:S(2)}) copy-start(f32[256]{0:T(256)} %param.38) | copy-start | bytes 3076
  270.1 21.4 %copy-start.11 = (f32[256]{0:T(256)S(1)}, f32[256]{0:T(256)}, u32[]{:S(2)}) copy-start(f32[256]{0:T(256)} %param.37) | copy-start | bytes 3076
  296.2 30.2 %copy-start.10 = (f32[4096]{0:T(1024)S(1)}, f32[4096]{0:T(1024)}, u32[]{:S(2)}) copy-start(f32[4096]{0:T(1024)} %param.41) | copy-start | bytes 49156
  (5 other events, 9.5 us)
Sparse Core Ops, SparseCore 0:
  8.9 25.2 all-gather.4
  46.3 49.1 all-gather.6
  296.4 28.7 reduce-scatter.1
where the time goes:
time: 339 us; the launch traced here: 335 us
  local copies, waits for them, and re-layouts  107 us (32%)
  blocking collectives  74 us (22%)
  other arithmetic  55.4 us (16%)
  waiting for transfers between devices  52.6 us (16%)
  matrix products  27.6 us (8%)
  between operations  13.5 us (4%)
  starting transfers between devices  4.15 us (1%)
    slice x52, local copies, waits for them, and re-layouts, shards(): lax.associative_scan(combine_steps, (keep_rate, driven), axis=0)  64.7 us
    all_gather x2, blocking collectives, entering(): pieces = jax.tree.map(lambda part: lax.all_gather(part, axis), value)  34.8 us
    all_gather x1, blocking collectives, shards(): rope_source = lax.all_gather(rope_key, 'sp', axis=0, tiled=True)  33.6 us
    reduce_scatter x1, waiting for transfers between devices, shards(): lax.psum_scatter((jnp.dot(rec_norm, w_out_rec, preferred_element_type=jnp...  28.9 us
    pad x28, local copies, waits for them, and re-layouts, shards(): lax.associative_scan(combine_steps, (keep_rate, driven), axis=0)  25.2 us
    all_gather x1, waiting for transfers between devices, shards(): lax.all_gather(tokens, 'tp', axis=1, tiled=True).astype(jnp.float32)  23 us
    add x13, other arithmetic, combine_steps(): return (earlier[0] * later[0], later[0] * earlier[1] + later[1])  17.2 us
    dot_general x5, matrix products, accumulate(): return jnp.dot(source, weight, preferred_element_type=jnp.float32)  14.1 us
  transfers between devices with their start and end apart: 4, of which 2 were waited for; matrix products, arithmetic and copies ran while one was open for 48% of the time, Pallas kernels for 0%

commit v1 on v0

--- a/solution.py
+++ b/solution.py
@@ -11,6 +11,10 @@
 RATE_C = 8.0
 THETA = 10000.0
 span_limit = 2048
+
+
+def ratios_mix(mesh_dim, where_dim, sample):
+    return jnp.concatenate(lax.all_gather(sample, mesh_dim), axis=where_dim)
 
 
 def passed_along(block, axis, distance):
@@ -108,7 +112,7 @@
     first_place = lax.axis_index("sp") * row_count
     places = first_place + jnp.arange(row_count)
     last_place = first_place + row_count - 1
-    piece_wide = lax.all_gather(tokens, "tp", axis=1, tiled=True).astype(jnp.float32)
+    piece_wide = ratios_mix("tp", 1, sample=tokens).astype(jnp.float32)
     piece_low = (piece_wide * pre_gain).astype(jnp.bfloat16)
 
     def accumulate(source, weight):

time: 339 us -> 289 us (0.85)
  local copies, waits for them, and re-layouts: 107 us -> 71.5 us
  other arithmetic: 55.4 us -> 46.7 us
    slice x52, local copies, waits for them, and re-layouts: 64.7 us -> 25.5 us  [shards(): lax.associative_scan(combine_steps, (keep_rate, driven), axis=0)]
    add x13, other arithmetic: 17.2 us -> 8.49 us  [combine_steps(): return (earlier[0] * later[0], later[0] * earlier[1] + later[1])]
    convert_element_type x0 -> x1, local copies, waits for them, and re-layouts: none -> 5.38 us  [shards(): piece_wide = ratios_mix('tp', 1, sample=tokens).astype(jnp.float32)]
    pad x28, local copies, waits for them, and re-layouts: 25.2 us -> 19.9 us  [shards(): lax.associative_scan(combine_steps, (keep_rate, driven), axis=0)]
    convert_element_type x0 -> x2, other arithmetic: none -> 5.09 us  [the longest x1 2.64 us: shards(): piece_low = (piece_wide * pre_gain).astype(jnp.bfloat16)]
    dot_general x5, matrix products: 14.1 us -> 9.36 us  [accumulate(): return jnp.dot(source, weight, preferred_element_type=jnp.float32)]
    concatenate x14, other arithmetic: 11.1 us -> 7.12 us  [shards(): lax.associative_scan(combine_steps, (keep_rate, driven), axis=0)]
  transfers between devices with their start and end apart: 4 -> 4, of which waited for: 2 -> 2; matrix products, arithmetic and copies ran while one was open for 48% -> 35% of each run, Pallas kernels for 0% -> 0%
where the time goes in v1:
time: 289 us; the launch traced here: 287 us
  blocking collectives  73.4 us (25%)
  local copies, waits for them, and re-layouts  71.5 us (25%)
  waiting for transfers between devices  52.4 us (18%)
  other arithmetic  46.7 us (16%)
  matrix products  25 us (9%)
  between operations  13.6 us (5%)
  starting transfers between devices  4.03 us (1%)
    all_gather x2, blocking collectives, entering(): pieces = jax.tree.map(lambda part: lax.all_gather(part, axis), value)  34.8 us
    all_gather x1, blocking collectives, shards(): rope_source = lax.all_gather(rope_key, 'sp', axis=0, tiled=True)  32.8 us
    reduce_scatter x1, waiting for transfers between devices, shards(): lax.psum_scatter((jnp.dot(rec_norm, w_out_rec, preferred_element_type=jnp...  28.6 us
    slice x52, local copies, waits for them, and re-layouts, shards(): lax.associative_scan(combine_steps, (keep_rate, driven), axis=0)  25.5 us
    all_gather x1, waiting for transfers between devices, ratios_mix(): return jnp.concatenate(lax.all_gather(sample, mesh_dim), axis=where_dim)  23 us
    pad x28, local copies, waits for them, and re-layouts, shards(): lax.associative_scan(combine_steps, (keep_rate, driven), axis=0)  19.9 us
    dot_general x5, matrix products, accumulate(): return jnp.dot(source, weight, preferred_element_type=jnp.float32)  9.36 us
    add x13, other arithmetic, combine_steps(): return (earlier[0] * later[0], later[0] * earlier[1] + later[1])  8.49 us
  transfers between devices with their start and end apart: 4, of which 2 were waited for; matrix products, arithmetic and copies ran while one was open for 35% of the time, Pallas kernels for 0%

profile of v1, /device:TPU:0, one launch (start us, length us, event | category | flops | bytes accessed | tf_op | source)
XLA Modules:
  0.0 286.9 jit_solution(11076887305075248492)
XLA Ops:
  11.2 23.0 %all-gather.8.cloned.1.call-done = bf16[1024,1024]{1,0:T(8,128)(2,1)} async-done(((bf16[256,1024]{1,0:T(8,128)(2,1)}), bf16[1024,1024]{1,0:T(8,128)(2,1)}) %all-gather.8.cloned.1.call-update) | async-done | bytes 2097168 | tf_op jit(solution)/shard_map/all_gather | solution.py:17
  34.2 2.2 fusion.15
  36.5 2.4 convert_bitcast_fusion
  38.9 5.4 %copy.63 = f32[256,4,1024]{0,2,1:T(8,128)} copy(f32[256,4,1024]{2,0,1:T(8,128)} %convert_bitcast_fusion) | data formatting | bytes 8388608 | tf_op jit(solution)/shard_map/convert_element_type | solution.py:115
  44.3 2.6 fusion.16
  50.7 3.9 %collective-permute-start = (bf16[3,256]{1,0:T(4,128)(2,1)}, bf16[3,256]{1,0:T(4,128)(2,1)}, u32[]{:S(2)}, u32[]{:S(2)}) collective-permute-start(bf16[3,256]{1,0:T(4,128)(2,1)} %slice.384), channel_id=1, source_target_pairs={{0,4},{4,8},{8,12},{12,16},{16,20},{20,24},{24,28},{1,5},{5,9},{9,... | collective-permute-start | bytes 4616 | tf_op jit(solution)/shard_map/ppermute | solution.py:23
  55.5 32.8 %all_gather.23 = bf16[2048,64]{0,1:T(8,128)(2,1)} all-gather(bf16[256,64]{0,1:T(8,128)(2,1)S(1)} %pad_maximum_fusion.8), channel_id=1, replica_groups=mesh['sp'=8,'tp'=4] {'sp'}, dimensions={0}, use_global_device_ids=true | all-gather | bytes 294912 | tf_op jit(solution)/shard_map/all_gather | solution.py:178
  90.5 2.1 multiply_reduce_fusion
  95.0 2.3 convolution_convert_fusion
  108.5 2.1 multiply_multiply_fusion.1
  160.5 2.2 pad.110
  162.7 2.2 pad.111
  164.9 2.2 pad.127
  176.0 2.3 pad.113
  179.1 17.7 %all-gather.2 = f32[8,1,256]{2,1,0:T(1,128)S(1)} all-gather(f32[1,1,256]{2,1,0:T(1,128)S(1)} %add_bitcast_fusion), channel_id=1, replica_groups=mesh['sp'=8,'tp'=4] {'sp'}, dimensions={0}, use_global_device_ids=true | all-gather | bytes 9216 | tf_op jit(solution)/shard_map/all_gather | solution.py:28
  196.8 2.3 pad.129
  199.8 17.0 %all-gather.1 = f32[8,1,256]{2,1,0:T(1,128)S(1)} all-gather(f32[1,1,256]{2,1,0:T(1,128)S(1)} %add_bitcast_fusion.1), channel_id=1, replica_groups=mesh['sp'=8,'tp'=4] {'sp'}, dimensions={0}, use_global_device_ids=true | all-gather | bytes 9216 | tf_op jit(solution)/shard_map/all_gather | solution.py:28
  217.3 4.0 %multiply_reduce_fusion.1 = (f32[256]{0:T(256)S(1)}, f32[256,256]{1,0:T(8,128)}) fusion(bf16[256,4096]{0,1:T(8,128)(2,1)} %copy-done.1, bf16[4096,256]{1,0:T(8,128)(2,1)} %param.27, f32[256]{0:T(256)S(1)} %copy-done.17, f32[256]{0:T(256)S(1)} %get-tuple-element.224, f32[256,256]{1,0:T(8,128)} %pad.128, f32[256,256]{1,0:T(8,128)} %pad.129, ...), kind=kOutput, calls=%fused_computation.68 | convolution fusion | flops 537919232 | bytes 5508096 | tf_op jit(solution)/shard_map/dot_general | solution.py:119
  221.3 15.4 %conditional.1 = (f32[2,256]{1,0:T(2,128)S(1)}, f32[2,256,128]{1,2,0:T(8,128)}) conditional(s32[]{:T(128)} %convert_element_type.94, (f32[2,256]{1,0:T(2,128)S(1)}, f32[2,256,128]{2,1,0:T(8,128)S(1)}) %tuple.114, (s32[]{:T(128)}, s32[256]{0:T(256)S(1)}, bf16[2048,512]{1,0:T(8,128)(2,1)}, f32[256,2,192]{0,2,1:T(8,128)}, bf16[2048,64]{0,1:T(8,128)(2,1)}, ...), branch_computations={%region_6.7_spmd, %region_7.10_spmd} | conditional | flops 680135424 | bytes 41970792 | solution.py:204
  224.4 3.9 %copy.72 = bf16[2048,512]{0,1:T(8,128)(2,1)} copy(bf16[2048,512]{1,0:T(8,128)(2,1)} %get-tuple-element.273) | data formatting | bytes 4194304 | tf_op jit(solution)/shard_map
  237.7 5.9 %all-reduce.32 = (f32[256,1]{0,1:T(1,128)S(1)}, f32[256,1]{0,1:T(1,128)S(1)}) all-reduce(f32[256,1]{0,1:T(1,128)S(1)} %bitcast.105, f32[256,1]{0,1:T(1,128)S(1)} %bitcast.99), channel_id=1, replica_groups=mesh['sp'=8,'tp'=4] {'tp'}, use_global_device_ids=true, to_apply=%region_4.5 | all-reduce | flops 512 | bytes 4096 | tf_op jit(solution)/shard_map/psum | solution.py:211
  243.7 2.6 fusion.43
  246.3 2.1 fusion.14
  248.5 28.6 %reduce-scatter.2.cloned.1.call-done = bf16[64,4096]{1,0:T(8,128)(2,1)} async-done(((bf16[256,4096]{1,0:T(8,128)(2,1)}), bf16[64,4096]{1,0:T(8,128)(2,1)}) %reduce-scatter.2.cloned.1.call-update) | async-done | bytes 524304 | tf_op jit(solution)/shard_map/reduce_scatter | solution.py:218
  (242 shorter events, 101.5 us)
Async XLA Ops:
  6.5 81.7 %copy-start = (bf16[4096,384]{1,0:T(8,128)(2,1)S(1)}, bf16[4096,384]{1,0:T(8,128)(2,1)}, u32[]{:S(2)}) copy-start(bf16[4096,384]{1,0:T(8,128)(2,1)} %param.32) | copy-start | bytes 9437188
  6.5 27.7 %all-gather.8.cloned.1.call-start = ((), (), s32[]{:S(2)}) async-start(), calls=%async_computation.3 | async-start | bytes 2621440 | tf_op jit(solution)/shard_map/all_gather | solution.py:17
  7.3 214.0 %all-gather.6.cloned.1.call-start = ((), (), s32[]{:S(2)}) async-start(), calls=%async_computation.1 | async-start | bytes 2359296 | tf_op jit(solution)/shard_map/all_gather | solution.py:177
  36.5 53.9 %copy-start.16 = (f32[256]{0:T(256)}, f32[256]{0:T(256)S(1)}, u32[]{:S(2)}) copy-start(f32[256]{0:T(256)S(1)} %add_rsqrt_fusion.3) | copy-start | bytes 3076
  38.9 5.4 %copy-start.14 = (f32[4096]{0:T(1024)S(1)}, f32[4096]{0:T(1024)}, u32[]{:S(2)}) copy-start(f32[4096]{0:T(1024)} %param.24) | copy-start | bytes 49156
  44.3 2.7 copy-start.9
  47.0 43.4 %copy-start.1 = (bf16[256,4096]{0,1:T(8,128)(2,1)}, bf16[256,4096]{0,1:T(8,128)(2,1)S(1)}, u32[]{:S(2)}) copy-start(bf16[256,4096]{0,1:T(8,128)(2,1)S(1)} %fusion.16) | copy-start | bytes 6291460
  47.0 2.4 copy-start.27
  49.3 5.3 %copy-start.24 = (f32[256]{0:T(256)S(1)}, f32[256]{0:T(256)}, u32[]{:S(2)}) copy-start(f32[256]{0:T(256)} %add_convert_fusion.2) | copy-start | bytes 3076
  49.3 5.3 %copy-start.25 = (f32[32]{0:T(128)S(1)}, f32[32]{0:T(128)}, u32[]{:S(2)}) copy-start(f32[32]{0:T(128)} %negate_power_fusion) | copy-start | bytes 388
  50.7 48.2 %collective-permute-start = (bf16[3,256]{1,0:T(4,128)(2,1)}, bf16[3,256]{1,0:T(4,128)(2,1)}, u32[]{:S(2)}, u32[]{:S(2)}) collective-permute-start(bf16[3,256]{1,0:T(4,128)(2,1)} %slice.384), channel_id=1, source_target_pairs={{0,4},{4,8},{8,12},{12,16},{16,20},{20,24},{24,28},{1,5},{5,9},{9,... | collective-permute-start | bytes 4616 | tf_op jit(solution)/shard_map/ppermute | solution.py:23
  92.5 6.4 %copy-start.22 = (f32[1,256]{1,0:T(1,128)S(1)}, f32[1,256]{1,0:T(1,128)}, u32[]{:S(2)}) copy-start(f32[1,256]{1,0:T(1,128)} %get-tuple-element.339) | copy-start | bytes 3076
  97.3 179.8 %reduce-scatter.2.cloned.1.call-start = ((), (), s32[]{:S(2)}) async-start(), calls=%async_computation.2 | async-start | bytes 2621440 | tf_op jit(solution)/shard_map/reduce_scatter | solution.py:218
  142.9 16.1 %copy-start.21 = (f32[1,256]{1,0:T(1,128)S(1)}, f32[1,256]{1,0:T(1,128)}, u32[]{:S(2)}) copy-start(f32[1,256]{1,0:T(1,128)} %slice.390) | copy-start | bytes 3076
  146.2 25.9 %copy-start.20 = (f32[1,256]{1,0:T(1,128)S(1)}, f32[1,256]{1,0:T(1,128)}, u32[]{:S(2)}) copy-start(f32[1,256]{1,0:T(1,128)} %slice.415) | copy-start | bytes 3076
  153.9 19.8 %copy-start.19 = (f32[1,256]{1,0:T(1,128)S(1)}, f32[1,256]{1,0:T(1,128)}, u32[]{:S(2)}) copy-start(f32[1,256]{1,0:T(1,128)} %slice.389) | copy-start | bytes 3076
  164.9 52.0 %copy-start.12 = (f32[256]{0:T(256)S(1)}, f32[256]{0:T(256)}, u32[]{:S(2)}) copy-start(f32[256]{0:T(256)} %custom-call) | copy-start | bytes 3076
  167.1 50.2 %copy-start.17 = (f32[256]{0:T(256)S(1)}, f32[256]{0:T(256)}, u32[]{:S(2)}) copy-start(f32[256]{0:T(256)} %copy-done.16) | copy-start | bytes 3076
  217.2 4.0 %copy-start.10 = (bf16[256,2,64]{0,2,1:T(8,128)(2,1)S(1)}, bf16[256,2,64]{0,2,1:T(8,128)(2,1)}, u32[]{:S(2)}) copy-start(bf16[256,2,64]{0,2,1:T(8,128)(2,1)} %pad_maximum_fusion.5) | copy-start | bytes 196612
  217.3 4.0 %copy-start.13 = (f32[2,256]{1,0:T(2,128)S(1)}, f32[2,256]{1,0:T(2,128)}, u32[]{:S(2)}) copy-start(f32[2,256]{1,0:T(2,128)} %broadcast_in_dim.63) | copy-start | bytes 6148
  221.3 22.3 %copy-start.23 = (f32[256]{0:T(256)S(1)}, f32[256]{0:T(256)}, u32[]{:S(2)}) copy-start(f32[256]{0:T(256)} %param.38) | copy-start | bytes 3076
  221.3 22.4 %copy-start.18 = (f32[256]{0:T(256)S(1)}, f32[256]{0:T(256)}, u32[]{:S(2)}) copy-start(f32[256]{0:T(256)} %param.37) | copy-start | bytes 3076
  243.7 2.6 copy-start.5
  248.4 29.9 %copy-start.15 = (f32[4096]{0:T(1024)S(1)}, f32[4096]{0:T(1024)}, u32[]{:S(2)}) copy-start(f32[4096]{0:T(1024)} %param.41) | copy-start | bytes 49156
  (8 other events, 12.2 us)
Sparse Core Ops, SparseCore 0:
  8.9 25.2 all-gather.7
  97.5 46.3 all-gather.5
  248.6 28.4 reduce-scatter.1
